TPU v7x, 32 devices: a whole 2x2x4 slice. The times are simulated.
32 devices in a mesh: rep: 2 (over y), fs: 4 (over z), tp: 4 (over x, core).
Axes of the slice: x: 2, y: 2, z: 4, core: 2. Of those that a mesh axis runs over, the one named last changes fastest.
Arguments:
- tokens: bfloat16 [2048, 2048], P(('rep', 'fs')), may hold values from -6 to 6
- gate_weight: bfloat16 [2048, 2816], P('fs', 'tp'), may hold values from -0.125 to 0.125
- up_weight: bfloat16 [2048, 2816], P('fs', 'tp'), may hold values from -0.125 to 0.125
- down_weight: bfloat16 [2816, 2048], P('tp', 'fs'), may hold values from -0.109375 to 0.109375
- out_grad: bfloat16 [2048, 2048], P(('rep', 'fs')), may hold values from -6 to 6
Outputs:
- input_grad: bfloat16 [2048, 2048], P(('rep', 'fs'))
- down_grad: float32 [2816, 2048], P('tp', 'fs')
- row_norms: float32 [2816], P('tp')
All inputs are finite; a program needn't handle non-finite values.
Results may differ from a plain program's by a relative error of at most 0.024.
Values may be sent and summed in bfloat16 or wider, within the bound.
A program may use at most 64 MiB of HBM per device.

v0:
```python
import jax
import jax.numpy as jnp
from jax import lax
from jax.sharding import PartitionSpec as P


def contract_last(left, right):
    return lax.dot_general(
        left, right, (((1,), (1,)), ((), ())), preferred_element_type=jnp.float32
    )


def contract_first(left, right):
    return lax.dot_general(
        left, right, (((0,), (0,)), ((), ())), preferred_element_type=jnp.float32
    )


def on_device(tokens, gate_weight, up_weight, down_weight, out_grad):
    down_full = lax.all_gather(down_weight, "fs", axis=1, tiled=True)
    gate_full, up_full = (
        lax.all_gather(gate_weight, "fs", axis=0, tiled=True),
        lax.all_gather(up_weight, "fs", axis=0, tiled=True),
    )
    gate_pre = jnp.dot(tokens, gate_full, preferred_element_type=jnp.float32)
    up_pre = jnp.dot(tokens, up_full, preferred_element_type=jnp.float32)
    sigma = jax.nn.sigmoid(gate_pre)
    activated = gate_pre * sigma
    hidden = (activated * up_pre).astype(jnp.bfloat16)
    hid_grad = contract_last(out_grad, down_full)
    up_grad = (hid_grad * activated).astype(jnp.bfloat16)
    gate_grad = (hid_grad * up_pre * sigma * (1.0 + gate_pre * (1.0 - sigma))).astype(jnp.bfloat16)
    partial_value = contract_last(gate_grad, gate_full) + contract_last(up_grad, up_full)
    input_grad = lax.psum(partial_value.astype(jnp.bfloat16), "tp")
    columns = lax.all_to_all(out_grad, "fs", split_axis=1, concat_axis=0, tiled=True)
    shard = contract_first(lax.all_gather(hidden, "fs", axis=0, tiled=True), columns)
    shard = lax.psum(shard.astype(jnp.bfloat16), "rep").astype(jnp.float32)
    norms = lax.psum(jnp.sum(shard * shard, axis=1), "fs")
    return (input_grad, shard, norms)


def solution(mesh):
    return jax.shard_map(
        on_device,
        mesh=mesh,
        in_specs=(
            P(("rep", "fs"), None),
            P("fs", "tp"),
            P("fs", "tp"),
            P("tp", "fs"),
            P(("rep", "fs"), None),
        ),
        out_specs=(P(("rep", "fs"), None), P("tp", "fs"), P("tp")),
        check_vma=False,
    )
```

profile of v0, /device:TPU:0, one launch (start us, length us, event | category | flops | bytes accessed | tf_op | source)
XLA Modules:
  0.0 329.1 jit_solution(854777100918134661)
XLA Ops:
  7.2 0.7 all-gather.9.cloned.1.call-update
  8.0 0.7 all-gather.7.cloned.1.call-update
  8.7 0.7 all-gather.5.cloned.1.call-update
  9.4 0.0 all-gather.11.cloned.1.call-start
  9.4 62.0 %all-gather.9.cloned.1.call-done = bf16[2048,704]{0,1:T(8,128)(2,1)} async-done(((bf16[512,704]{0,1:T(8,128)(2,1)}), bf16[2048,704]{0,1:T(8,128)(2,1)}) %all-gather.9.cloned.1.call-update) | async-done | bytes 2883600 | tf_op jit(solution)/shard_map/all_gather | solution.py:22
  71.4 2.8 fusion.8
  74.2 56.6 %all-gather.7.cloned.1.call-done = bf16[2048,704]{0,1:T(8,128)(2,1)} async-done(((bf16[512,704]{0,1:T(8,128)(2,1)}), bf16[2048,704]{0,1:T(8,128)(2,1)}) %all-gather.7.cloned.1.call-update) | async-done | bytes 2883600 | tf_op jit(solution)/shard_map/all_gather | solution.py:23
  130.8 3.7 %multiply_convert_fusion = (bf16[256,704]{0,1:T(8,128)(2,1)}, f32[256,704]{0,1:T(8,128)}) fusion(f32[256,704]{0,1:T(8,128)S(1)} %fusion.8, bf16[256,2048]{1,0:T(8,128)(2,1)S(1)} %copy-done, bf16[2048,704]{0,1:T(8,128)(2,1)} %all-gather.7.cloned.1.call-done), kind=kOutput, calls=%fused_computation.4 | convolution fusion | flops 739278848 | bytes 5734400 | tf_op jit(solution)/shard_map/dot_general | solution.py:26
  134.6 0.0 all-reduce.5.cloned.1.call-start
  134.7 0.5 copy.8
  135.2 56.6 %all_to_all.19 = bf16[256,4,512]{0,2,1:T(8,128)(2,1)S(1)} all-to-all(bf16[256,4,512]{0,2,1:T(8,128)(2,1)S(1)} %bitcast.14), channel_id=1, replica_groups=mesh['rep'=2,'fs'=4,'tp'=4] {'fs'}, dimensions={1} | all-to-all | bytes 2097152 | tf_op jit(solution)/shard_map/all_to_all | solution.py:35
  191.8 0.5 copy.9
  192.4 17.8 %all-gather.5.cloned.1.call-done = bf16[704,2048]{1,0:T(8,128)(2,1)} async-done(((bf16[704,512]{1,0:T(8,128)(2,1)}), bf16[704,2048]{1,0:T(8,128)(2,1)}) %all-gather.5.cloned.1.call-update) | async-done | bytes 2883600 | tf_op jit(solution)/shard_map/all_gather | solution.py:20
  210.1 3.9 %fusion.7 = f32[256,704]{0,1:T(8,128)} fusion(bf16[256,2048]{1,0:T(8,128)(2,1)} %param.9, bf16[704,2048]{1,0:T(8,128)(2,1)} %all-gather.5.cloned.1.call-done), kind=kOutput, calls=%fused_computation.13 | convolution fusion | flops 738197504 | bytes 4653056 | tf_op jit(solution)/shard_map/dot_general | solution.py:8
  214.1 32.2 %all-gather.11.cloned.1.call-done = bf16[1024,704]{0,1:T(8,128)(2,1)} async-done(((bf16[256,704]{0,1:T(8,128)(2,1)}), bf16[1024,704]{0,1:T(8,128)(2,1)}) %all-gather.11.cloned.1.call-update) | async-done | bytes 1441808 | tf_op jit(solution)/shard_map/all_gather | solution.py:36
  246.3 3.2 convolution_convert_fusion
  249.5 0.0 all-reduce.3.cloned.1.call-start
  249.6 3.5 %fusion.2 = f32[256,2048]{1,0:T(8,128)S(1)} fusion(bf16[2048,704]{0,1:T(8,128)(2,1)} %all-gather.9.cloned.1.call-done, f32[256,704]{0,1:T(8,128)S(1)} %copy-done.4, f32[256,704]{0,1:T(8,128)} %fusion.7, f32[256,704]{0,1:T(8,128)} %get-tuple-element.6), kind=kOutput, calls=%fused_computation.9 | convolution fusion | flops 739999744 | bytes 7143424 | tf_op jit(solution)/shard_map/dot_general | solution.py:8
  253.1 2.0 fusion
  255.2 25.6 %all-reduce.5.cloned.1.call-done = bf16[704,512]{1,0:T(8,128)(2,1)} async-done(((bf16[704,512]{1,0:T(8,128)(2,1)}), bf16[704,512]{1,0:T(8,128)(2,1)}) %all-reduce.5.cloned.1.call-update) | async-done | bytes 720912 | tf_op jit(solution)/shard_map/psum | solution.py:37
  280.8 2.3 multiply_reduce_fusion
  283.1 12.2 %psum.23 = f32[704]{0:T(1024)} all-reduce(f32[704]{0:T(1024)S(1)} %get-tuple-element.3), channel_id=1, replica_groups=mesh['rep'=2,'fs'=4,'tp'=4] {'fs'}, use_global_device_ids=true, to_apply=%region_3.0 | all-reduce | flops 704 | bytes 5632 | tf_op jit(solution)/shard_map/psum | solution.py:38
  295.4 24.5 %all-reduce.3.cloned.1.call-done = bf16[256,2048]{1,0:T(8,128)(2,1)} async-done(((bf16[256,2048]{1,0:T(8,128)(2,1)}), bf16[256,2048]{1,0:T(8,128)(2,1)}) %all-reduce.3.cloned.1.call-update) | async-done | bytes 1048592 | tf_op jit(solution)/shard_map/psum | solution.py:34
  319.9 2.3 copy.12
  (18 shorter events, 0.2 us)
Async XLA Ops:
  7.2 64.3 %copy-start = (bf16[256,2048]{1,0:T(8,128)(2,1)S(1)}, bf16[256,2048]{1,0:T(8,128)(2,1)}, u32[]{:S(2)}) copy-start(bf16[256,2048]{1,0:T(8,128)(2,1)} %param.5) | copy-start | bytes 3145732
  7.2 64.2 %all-gather.9.cloned.1.call-start = ((), (), s32[]{:S(2)}) async-start(), calls=%async_computation.3 | async-start | bytes 3604480 | tf_op jit(solution)/shard_map/all_gather | solution.py:22
  7.9 122.9 %all-gather.7.cloned.1.call-start = ((), (), s32[]{:S(2)}) async-start(), calls=%async_computation.2 | async-start | bytes 3604480 | tf_op jit(solution)/shard_map/all_gather | solution.py:23
  8.7 201.5 %all-gather.5.cloned.1.call-start = ((), (), s32[]{:S(2)}) async-start(), calls=%async_computation.1 | async-start | bytes 3604480 | tf_op jit(solution)/shard_map/all_gather | solution.py:20
  9.4 236.9 %all-gather.11.cloned.1.call-start = ((), (), s32[]{:S(2)}) async-start(), calls=%async_computation.5 | async-start | bytes 1802240 | tf_op jit(solution)/shard_map/all_gather | solution.py:36
  74.2 60.4 %copy-start.3 = (f32[256,704]{0,1:T(8,128)}, f32[256,704]{0,1:T(8,128)S(1)}, u32[]{:S(2)}) copy-start(f32[256,704]{0,1:T(8,128)S(1)} %fusion.8) | copy-start | bytes 2162692
  74.2 60.4 %copy-start.2 = (bf16[256,2048]{1,0:T(8,128)(2,1)S(1)}, bf16[256,2048]{1,0:T(8,128)(2,1)}, u32[]{:S(2)}) copy-start(bf16[256,2048]{1,0:T(8,128)(2,1)} %param.9) | copy-start | bytes 3145732
  134.6 146.2 %all-reduce.5.cloned.1.call-start = ((), (), s32[]{:S(2)}) async-start(), calls=%async_computation.6 | async-start | bytes 1441792 | tf_op jit(solution)/shard_map/psum | solution.py:37
  246.3 3.3 %copy-start.4 = (f32[256,704]{0,1:T(8,128)S(1)}, f32[256,704]{0,1:T(8,128)}, u32[]{:S(2)}) copy-start(f32[256,704]{0,1:T(8,128)} %copy-done.3) | copy-start | bytes 2162692
  249.5 70.4 %all-reduce.3.cloned.1.call-start = ((), (), s32[]{:S(2)}) async-start(), calls=%async_computation.4 | async-start | bytes 2097152 | tf_op jit(solution)/shard_map/psum | solution.py:34
  249.6 3.5 %copy-start.1 = (bf16[2048,704]{0,1:T(8,128)(2,1)S(1)}, bf16[2048,704]{0,1:T(8,128)(2,1)}, u32[]{:S(2)}) copy-start(bf16[2048,704]{0,1:T(8,128)(2,1)} %all-gather.7.cloned.1.call-done) | copy-start | bytes 8650756
  249.6 3.5 %copy-start.5 = (f32[256,704]{0,1:T(8,128)S(1)}, f32[256,704]{0,1:T(8,128)}, u32[]{:S(2)}) copy-start(f32[256,704]{0,1:T(8,128)} %fusion.7) | copy-start | bytes 2162692
Sparse Core Ops, SparseCore 0:
  9.6 61.8 all-gather.8
  73.0 57.7 all-gather.6
  132.4 77.6 all-gather.4
  211.6 34.6 all-gather.10
  249.6 31.1 all-reduce.4
  283.6 36.2 all-reduce.2
where the time goes:
time: 329 us
  waiting for transfers between devices  221 us (67%)
  blocking collectives  68.9 us (21%)
  matrix products  19.2 us (6%)
  between operations  14.2 us (4%)
  local copies, waits for them, and re-layouts  3.4 us (1%)
    all_gather x1, waiting for transfers between devices, on_device(): lax.all_gather(gate_weight, 'fs', axis=0, tiled=True)  62 us
    all_to_all x1, blocking collectives, on_device(): lax.all_to_all(out_grad, 'fs', split_axis=1, concat_axis=0, tiled=True)  56.6 us
    all_gather x1, waiting for transfers between devices, on_device(): lax.all_gather(up_weight, 'fs', axis=0, tiled=True)  56.6 us
    all_gather x1, waiting for transfers between devices, on_device(): lax.all_gather(hidden, 'fs', axis=0, tiled=True)  32.2 us
    psum x1, waiting for transfers between devices, on_device(): shard = lax.psum(shard.astype(jnp.bfloat16), 'rep').astype(jnp.float32)  25.6 us
    psum x1, waiting for transfers between devices, on_device(): input_grad = lax.psum(partial_value.astype(jnp.bfloat16), 'tp')  24.5 us
    all_gather x1, waiting for transfers between devices, on_device(): down_full = lax.all_gather(down_weight, 'fs', axis=1, tiled=True)  17.8 us
    psum x1, blocking collectives, on_device(): norms = lax.psum(jnp.sum(shard * shard, axis=1), 'fs')  12.2 us
  transfers between devices with their start and end apart: 6, of which 6 were waited for; matrix products, arithmetic and copies ran while one was open for 6% of the time, Pallas kernels for 0%

commit v1 on v0

--- a/solution.py
+++ b/solution.py
@@ -2,6 +2,12 @@
 import jax.numpy as jnp
 from jax import lax
 from jax.sharding import PartitionSpec as P
+
+
+def gather_and_add(block, axis):
+    parts = lax.all_gather(block, axis, axis=0, tiled=False)
+    total = parts.sum(axis=0)
+    return total
 
 
 def contract_last(left, right):
@@ -34,7 +40,7 @@
     input_grad = lax.psum(partial_value.astype(jnp.bfloat16), "tp")
     columns = lax.all_to_all(out_grad, "fs", split_axis=1, concat_axis=0, tiled=True)
     shard = contract_first(lax.all_gather(hidden, "fs", axis=0, tiled=True), columns)
-    shard = lax.psum(shard.astype(jnp.bfloat16), "rep").astype(jnp.float32)
+    shard = gather_and_add(shard.astype(jnp.bfloat16), "rep").astype(jnp.float32)
     norms = lax.psum(jnp.sum(shard * shard, axis=1), "fs")
     return (input_grad, shard, norms)
 

time: 329 us -> 322 us (0.979)
  blocking collectives: 68.9 us -> 62.6 us
  matrix products: 19.2 us -> 15.9 us
    all_gather x1, waiting for transfers between devices: 17.8 us -> 56.3 us  [on_device(): down_full = lax.all_gather(down_weight, 'fs', axis=1, tiled=True)]
    all_gather x1, waiting for transfers between devices: 32.2 us -> 0.83 us  [on_device(): lax.all_gather(hidden, 'fs', axis=0, tiled=True)]
    psum x1 -> x0, waiting for transfers between devices: 25.6 us -> none  [on_device(): shard = lax.psum(shard.astype(jnp.bfloat16), 'rep').astype(jnp.float32)]
    all_gather x0 -> x1, waiting for transfers between devices: none -> 19 us  [gather_and_add(): parts = lax.all_gather(block, axis, axis=0, tiled=False)]
    all_to_all x1, blocking collectives: 56.6 us -> 50.3 us  [on_device(): lax.all_to_all(out_grad, 'fs', split_axis=1, concat_axis=0, tiled=True)]
    dot_general x3, matrix products: 9.5 us -> 6.15 us  [contract_last(): lax.dot_general(left, right, (((1,), (1,)), ((), ())), preferred_element_...]
  transfers between devices with their start and end apart: 6 -> 6, of which waited for: 6 -> 6; matrix products, arithmetic and copies ran while one was open for 6% -> 5% of each run, Pallas kernels for 0% -> 0%
where the time goes in v1:
time: 322 us; the launch traced here: 321 us
  waiting for transfers between devices  221 us (69%)
  blocking collectives  62.6 us (19%)
  matrix products  15.9 us (5%)
  between operations  14.2 us (4%)
  local copies, waits for them, and re-layouts  4.01 us (1%)
  other arithmetic  3.25 us (1%)
    all_gather x1, waiting for transfers between devices, on_device(): lax.all_gather(gate_weight, 'fs', axis=0, tiled=True)  62.7 us
    all_gather x1, waiting for transfers between devices, on_device(): lax.all_gather(up_weight, 'fs', axis=0, tiled=True)  56.6 us
    all_gather x1, waiting for transfers between devices, on_device(): down_full = lax.all_gather(down_weight, 'fs', axis=1, tiled=True)  56.3 us
    all_to_all x1, blocking collectives, on_device(): lax.all_to_all(out_grad, 'fs', split_axis=1, concat_axis=0, tiled=True)  50.3 us
    psum x1, waiting for transfers between devices, on_device(): input_grad = lax.psum(partial_value.astype(jnp.bfloat16), 'tp')  23.6 us
    all_gather x1, waiting for transfers between devices, gather_and_add(): parts = lax.all_gather(block, axis, axis=0, tiled=False)  19 us
    psum x1, blocking collectives, on_device(): norms = lax.psum(jnp.sum(shard * shard, axis=1), 'fs')  12.2 us
  transfers between devices with their start and end apart: 6, of which 6 were waited for; matrix products, arithmetic and copies ran while one was open for 5% of the time, Pallas kernels for 0%

profile of v1, /device:TPU:0, one launch (start us, length us, event | category | flops | bytes accessed | tf_op | source)
XLA Modules:
  0.0 321.2 jit_solution(5377244753286905708)
XLA Ops:
  7.2 0.7 all-gather.11.cloned.1.call-update
  8.0 0.7 all-gather.9.cloned.1.call-update
  8.7 62.7 %all-gather.11.cloned.1.call-done = bf16[2048,704]{0,1:T(8,128)(2,1)} async-done(((bf16[512,704]{0,1:T(8,128)(2,1)}), bf16[2048,704]{0,1:T(8,128)(2,1)}) %all-gather.11.cloned.1.call-update) | async-done | bytes 2883600 | tf_op jit(solution)/shard_map/all_gather | solution.py:28
  71.4 2.8 fusion.8
  74.2 56.6 %all-gather.9.cloned.1.call-done = bf16[2048,704]{0,1:T(8,128)(2,1)} async-done(((bf16[512,704]{0,1:T(8,128)(2,1)}), bf16[2048,704]{0,1:T(8,128)(2,1)}) %all-gather.9.cloned.1.call-update) | async-done | bytes 2883600 | tf_op jit(solution)/shard_map/all_gather | solution.py:29
  130.8 3.8 %multiply_convert_fusion = (bf16[256,704]{0,1:T(8,128)(2,1)}, f32[256,704]{0,1:T(8,128)}) fusion(f32[256,704]{0,1:T(8,128)S(1)} %fusion.8, bf16[256,2048]{1,0:T(8,128)(2,1)S(1)} %copy-done, bf16[2048,704]{0,1:T(8,128)(2,1)} %all-gather.9.cloned.1.call-done), kind=kOutput, calls=%fused_computation.4 | convolution fusion | flops 739278848 | bytes 5734400 | tf_op jit(solution)/shard_map/dot_general | solution.py:32
  134.7 0.5 all-gather.7.cloned.1.call-update
  135.2 0.5 copy.8
  135.8 50.3 %all_to_all.19 = bf16[256,4,512]{0,2,1:T(8,128)(2,1)S(1)} all-to-all(bf16[256,4,512]{0,2,1:T(8,128)(2,1)S(1)} %bitcast.15), channel_id=1, replica_groups=mesh['rep'=2,'fs'=4,'tp'=4] {'fs'}, dimensions={1} | all-to-all | bytes 2097152 | tf_op jit(solution)/shard_map/all_to_all | solution.py:41
  186.1 0.5 copy.9
  186.6 0.8 all-gather.13.cloned.1.call-done
  187.5 3.2 %convolution_convert_fusion = bf16[704,512]{1,0:T(8,128)(2,1)} fusion(bf16[1024,704]{0,1:T(8,128)(2,1)} %all-gather.13.cloned.1.call-done, bf16[1024,512]{1,0:T(8,128)(2,1)S(1)} %bitcast.17), kind=kOutput, calls=%fused_computation.3 | convolution fusion | flops 738557952 | bytes 3211264 | tf_op jit(solution)/shard_map/dot_general | solution.py:20
  190.7 0.0 all-reduce.2.cloned.1.call-start
  190.8 56.3 %all-gather.7.cloned.1.call-done = bf16[704,2048]{1,0:T(8,128)(2,1)} async-done(((bf16[704,512]{1,0:T(8,128)(2,1)}), bf16[704,2048]{1,0:T(8,128)(2,1)}) %all-gather.7.cloned.1.call-update) | async-done | bytes 2883600 | tf_op jit(solution)/shard_map/all_gather | solution.py:26
  247.1 2.9 fusion.7
  250.1 1.2 fusion.2
  251.3 0.6 copy-done.1
  251.9 2.0 fusion
  254.0 19.0 %all-gather.15.cloned.1.call-done = bf16[1408,512]{1,0:T(8,128)(2,1)} async-done(((bf16[704,512]{1,0:T(8,128)(2,1)}), bf16[1408,512]{1,0:T(8,128)(2,1)}) %all-gather.15.cloned.1.call-update) | async-done | bytes 1441808 | tf_op jit(solution)/shard_map/all_gather | solution.py:8
  272.9 2.0 reduce_sum.21
  275.0 1.2 multiply_reduce_fusion
  276.2 12.2 %psum.15 = f32[704]{0:T(1024)} all-reduce(f32[704]{0:T(1024)S(1)} %get-tuple-element.3), channel_id=1, replica_groups=mesh['rep'=2,'fs'=4,'tp'=4] {'fs'}, use_global_device_ids=true, to_apply=%region_3.0 | all-reduce | flops 704 | bytes 5632 | tf_op jit(solution)/shard_map/psum | solution.py:44
  288.4 23.6 %all-reduce.2.cloned.1.call-done = bf16[256,2048]{1,0:T(8,128)(2,1)} async-done(((bf16[256,2048]{1,0:T(8,128)(2,1)}), bf16[256,2048]{1,0:T(8,128)(2,1)}) %all-reduce.2.cloned.1.call-update) | async-done | bytes 1048592 | tf_op jit(solution)/shard_map/psum | solution.py:40
  312.1 2.3 copy.11
  (23 shorter events, 0.3 us)
Async XLA Ops:
  7.2 64.3 %copy-start = (bf16[256,2048]{1,0:T(8,128)(2,1)S(1)}, bf16[256,2048]{1,0:T(8,128)(2,1)}, u32[]{:S(2)}) copy-start(bf16[256,2048]{1,0:T(8,128)(2,1)} %param.5) | copy-start | bytes 3145732
  7.2 64.2 %all-gather.11.cloned.1.call-start = ((), (), s32[]{:S(2)}) async-start(), calls=%async_computation.3 | async-start | bytes 3604480 | tf_op jit(solution)/shard_map/all_gather | solution.py:28
  7.9 122.9 %all-gather.9.cloned.1.call-start = ((), (), s32[]{:S(2)}) async-start(), calls=%async_computation.2 | async-start | bytes 3604480 | tf_op jit(solution)/shard_map/all_gather | solution.py:29
  8.7 178.8 %all-gather.13.cloned.1.call-start = ((), (), s32[]{:S(2)}) async-start(), calls=%async_computation.5 | async-start | bytes 1802240 | tf_op jit(solution)/shard_map/all_gather | solution.py:42
  74.2 60.4 %copy-start.4 = (f32[256,704]{0,1:T(8,128)}, f32[256,704]{0,1:T(8,128)S(1)}, u32[]{:S(2)}) copy-start(f32[256,704]{0,1:T(8,128)S(1)} %fusion.8) | copy-start | bytes 2162692
  74.2 61.0 %copy-start.2 = (bf16[256,2048]{1,0:T(8,128)(2,1)S(1)}, bf16[256,2048]{1,0:T(8,128)(2,1)}, u32[]{:S(2)}) copy-start(bf16[256,2048]{1,0:T(8,128)(2,1)} %param.9) | copy-start | bytes 3145732
  134.6 112.5 %all-gather.7.cloned.1.call-start = ((), (), s32[]{:S(2)}) async-start(), calls=%async_computation.1 | async-start | bytes 3604480 | tf_op jit(solution)/shard_map/all_gather | solution.py:26
  135.2 137.8 %all-gather.15.cloned.1.call-start = ((), (), s32[]{:S(2)}) async-start(), calls=%async_computation.6 | async-start | bytes 2162688 | tf_op jit(solution)/shard_map/all_gather | solution.py:8
  187.5 59.7 %copy-start.3 = (bf16[256,2048]{1,0:T(8,128)(2,1)S(1)}, bf16[256,2048]{1,0:T(8,128)(2,1)}, u32[]{:S(2)}) copy-start(bf16[256,2048]{1,0:T(8,128)(2,1)} %param.9) | copy-start | bytes 3145732
  190.7 59.4 %copy-start.5 = (f32[256,704]{0,1:T(8,128)S(1)}, f32[256,704]{0,1:T(8,128)}, u32[]{:S(2)}) copy-start(f32[256,704]{0,1:T(8,128)} %copy-done.4) | copy-start | bytes 2162692
  190.7 59.4 %copy-start.7 = (f32[256,704]{0,1:T(8,128)S(1)}, f32[256,704]{0,1:T(8,128)}, u32[]{:S(2)}) copy-start(f32[256,704]{0,1:T(8,128)} %get-tuple-element.6) | copy-start | bytes 2162692
  190.7 121.3 %all-reduce.2.cloned.1.call-start = ((), (), s32[]{:S(2)}) async-start(), calls=%async_computation.4 | async-start | bytes 2097152 | tf_op jit(solution)/shard_map/psum | solution.py:40
  247.1 2.9 copy-start.6
  250.1 1.8 copy-start.1
Sparse Core Ops, SparseCore 0:
  9.6 61.8 all-gather.10
  73.0 57.7 all-gather.8
  134.7 52.6 all-gather.12
  188.9 58.1 all-gather.6
  248.5 24.3 all-gather.14
  275.7 36.2 all-reduce.1
